TPU v7x, 128 devices: a whole 4x4x4 slice. The times are simulated.
128 devices in a mesh: sp: 16 (over z, y), tp: 8 (over x, core).
Axes of the slice: x: 4, y: 4, z: 4, core: 2. Of those that a mesh axis runs over, the one named last changes fastest.
Arguments:
- resid: bfloat16 [16384, 2048], P(('sp', 'tp')), may hold values from -6 to 6
- query_nope: bfloat16 [16384, 2048], P('sp', 'tp'), may hold values from -18 to 18
- query_rope: bfloat16 [16384, 1024], P('sp', 'tp'), may hold values from -300 to 300
- latent: bfloat16 [16384, 256], P('sp'), may hold values from -6 to 6
- key_rope: bfloat16 [16384, 64], P('sp'), may hold values from -6 to 6
- latent_gain: float32 [256], replicated, may hold values from 0.1 to 1.9
- w_key: bfloat16 [256, 2048], P(None, 'tp'), may hold values from -0.375 to 0.375
- w_value: bfloat16 [256, 2048], P(None, 'tp'), may hold values from -0.375 to 0.375
- w_out: bfloat16 [2048, 2048], P('tp'), may hold values from -0.125 to 0.125
- mix_gain: float32 [2048], replicated, may hold values from 0.1 to 1.9
- w_gate: bfloat16 [2048, 5632], P('sp', 'tp'), may hold values from -0.125 to 0.125
- w_up: bfloat16 [2048, 5632], P('sp', 'tp'), may hold values from -0.125 to 0.125
- w_down: bfloat16 [2048, 5632], P('sp', 'tp'), may hold values from -0.078125 to 0.078125
Outputs:
- layer_out: bfloat16 [16384, 2048], P(('sp', 'tp'))
All inputs are finite; a program needn't handle non-finite values.
Results may differ from a plain program's by a relative error of at most 0.0095.
Values may be sent and summed in bfloat16 or wider, within the bound.
No kernel may reach another device: no remote copies, remote signals or barrier semaphores. Data moves between devices by JAX's collectives and lax.ppermute only.
A program may use at most 128 MiB of HBM per device.

v0:
```python
import jax
import jax.numpy as jnp
from jax import lax
from jax.sharding import PartitionSpec as P

NOPE = 128
ROPE = 64
VDIM = 128
norm_eps = 1e-06
masked_score = -1e30
theta_base = 10000.0


def in_one_piece(arrays, axis, dim, along):
    both = jnp.concatenate(arrays, axis=along)
    filled, at, gathered = (lax.all_gather(both, axis, axis=dim, tiled=True), 0, [])
    for a in arrays:
        gathered.append(lax.slice_in_dim(filled, at, at + a.shape[along], axis=along))
        at += a.shape[along]
    return tuple(gathered)


def split_up(array, dim, count):
    lengths = array.shape
    tiles = array.reshape(*lengths[:dim], count, lengths[dim] // count, *lengths[dim + 1 :])
    return jnp.moveaxis(tiles, dim, 0)


def summed_on_arrival(array, axis, dim):
    tiles = split_up(array, dim, lax.axis_size(axis))
    arrived = lax.all_to_all(tiles, axis, split_axis=0, concat_axis=0, tiled=True)
    return arrived.astype(jnp.float32).sum(axis=0)


def rotate(values_in, angle):
    half_width = values_in.shape[-1] // 2
    front_half = values_in[..., :half_width]
    back_half = values_in[..., half_width:]
    cosine = jnp.cos(angle)
    sine_part = jnp.sin(angle)
    return jnp.concatenate(
        [front_half * cosine - back_half * sine_part, back_half * cosine + front_half * sine_part],
        axis=-1,
    )


def angles(positions, full_width):
    half_width = full_width // 2
    frequency = theta_base ** (-2.0 * jnp.arange(half_width).astype(jnp.float32) / full_width)
    return positions[:, None] * frequency[None, :]


def rms_scale(values_in, gain):
    return (
        values_in
        * lax.rsqrt(jnp.mean(values_in * values_in, axis=-1, keepdims=True) + norm_eps)
        * gain
    )


def attend(fold_state, queries, key_block, value_block, rope_block, block_start):
    nope_query, rope_query, query_rows = queries
    running_max, weight_sum, accumulated = fold_state
    key_rows = block_start + jnp.arange(key_block.shape[0], dtype=jnp.int32)
    causal = key_rows[None, :] <= query_rows[:, None]
    scores = jnp.einsum("qhd,khd->hqk", nope_query, key_block, preferred_element_type=jnp.float32)
    scores = scores + jnp.einsum(
        "qhr,kr->hqk", rope_query, rope_block, preferred_element_type=jnp.float32
    )
    scores = jnp.where(causal[None], scores * (NOPE + ROPE) ** (-0.5), masked_score)
    new_max = jnp.maximum(running_max, jnp.max(scores, axis=-1))
    weights = jnp.where(causal[None], jnp.exp(scores - new_max[..., None]), 0.0)
    factor = jnp.exp(running_max - new_max)
    weight_sum = weight_sum * factor + jnp.sum(weights, axis=-1)
    accumulated = accumulated * factor[..., None] + jnp.einsum(
        "hqk,khd->hqd",
        weights.astype(jnp.bfloat16),
        value_block,
        preferred_element_type=jnp.float32,
    )
    return (new_max, weight_sum, accumulated)


def over_blocks(fold_state, arrays, last_query, step_fn, row_count):
    piece_rows = arrays[0].shape[0]
    candidates = [
        row_count * multiple
        for multiple in (4, 2, 1)
        if piece_rows % (row_count * multiple) == 0 and row_count * multiple <= 2048
    ]
    block_rows = candidates[0]
    block_count = piece_rows // block_rows
    stacked = tuple(
        (member.reshape((block_count, block_rows) + member.shape[1:]) for member in arrays)
    )

    def advance(state_in, indexed):
        block_index, blocks_now = indexed
        block_start = block_index * block_rows

        def compute(state_now):
            return step_fn(state_now, blocks_now, block_start)

        def unchanged(state_now):
            return state_now

        return (lax.cond(block_start <= last_query, compute, unchanged, state_in), None)

    result, ignored = lax.scan(
        advance, fold_state, (jnp.arange(block_count, dtype=jnp.int32), stacked)
    )
    return result


def on_device(
    resid,
    query_nope,
    query_rope,
    latent,
    key_rope,
    latent_gain,
    w_key,
    w_value,
    w_out,
    mix_gain,
    w_gate,
    w_up,
    w_down,
):
    row_count = query_nope.shape[0]
    head_count = query_nope.shape[1] // NOPE
    first_row = lax.axis_index("sp") * row_count
    query_rows = first_row + jnp.arange(row_count, dtype=jnp.int32)
    angle = angles(query_rows.astype(jnp.float32), ROPE)
    nope_query = query_nope.reshape(row_count, head_count, NOPE)
    rope_query = rotate(
        query_rope.astype(jnp.float32).reshape(row_count, head_count, ROPE), angle[:, None, :]
    ).astype(jnp.bfloat16)
    latent_normed = rms_scale(latent.astype(jnp.float32), latent_gain).astype(jnp.bfloat16)
    key_rotated = rotate(key_rope.astype(jnp.float32), angle).astype(jnp.bfloat16)
    queries = (nope_query, rope_query, query_rows)
    last_query = first_row + row_count - 1
    initial = (
        jnp.full((head_count, row_count), masked_score, jnp.float32),
        jnp.zeros((head_count, row_count), jnp.float32),
        jnp.zeros((head_count, row_count, VDIM), jnp.float32),
    )
    gate_full, up_full, down_full = in_one_piece((w_gate, w_up, w_down), "sp", 0, 1)

    def expand_block(state_now, blocks_now, block_start):
        latent_block, rope_block = blocks_now
        key_block = jnp.dot(latent_block, w_key, preferred_element_type=jnp.float32).astype(
            jnp.bfloat16
        )
        value_block = jnp.dot(latent_block, w_value, preferred_element_type=jnp.float32).astype(
            jnp.bfloat16
        )
        return attend(
            state_now,
            queries,
            key_block.reshape(-1, head_count, NOPE),
            value_block.reshape(-1, head_count, VDIM),
            rope_block,
            block_start,
        )

    final_state = over_blocks(
        initial,
        in_one_piece((latent_normed, key_rotated), "sp", 0, 1),
        last_query,
        expand_block,
        row_count,
    )
    head_out = (final_state[2] / final_state[1][..., None]).astype(jnp.bfloat16)
    out_heads = w_out.reshape(head_count, VDIM, w_out.shape[1])
    part_rows = head_out
    head_term = jnp.einsum("hqv,hvd->qd", part_rows, out_heads, preferred_element_type=jnp.float32)
    attention_proj = summed_on_arrival(
        lax.optimization_barrier(head_term.astype(jnp.bfloat16))
        .astype(jnp.float32)
        .astype(jnp.bfloat16),
        "tp",
        0,
    )
    stream = resid.astype(jnp.float32) + attention_proj
    normed = rms_scale(stream, mix_gain).astype(jnp.bfloat16)
    row_piece = lax.all_gather(normed, "tp", axis=0, tiled=True)
    gate_value = jnp.dot(row_piece, gate_full, preferred_element_type=jnp.float32)
    upward = jnp.dot(row_piece, up_full, preferred_element_type=jnp.float32)
    hidden = (jax.nn.silu(gate_value) * upward).astype(jnp.bfloat16)
    part_rows = hidden
    down_term = lax.dot_general(
        part_rows, down_full, (((1,), (1,)), ((), ())), preferred_element_type=jnp.float32
    )
    mixer_out = lax.psum_scatter(
        lax.optimization_barrier(down_term.astype(jnp.bfloat16))
        .astype(jnp.float32)
        .astype(jnp.bfloat16),
        "tp",
        scatter_dimension=0,
        tiled=True,
    ).astype(jnp.float32)
    return (stream + 0.5 * mixer_out).astype(jnp.bfloat16)


def solution(mesh):
    return jax.shard_map(
        on_device,
        mesh=mesh,
        in_specs=(
            P(("sp", "tp"), None),
            P("sp", "tp"),
            P("sp", "tp"),
            P("sp", None),
            P("sp", None),
            P(),
            P(None, "tp"),
            P(None, "tp"),
            P("tp", None),
            P(),
            P("sp", "tp"),
            P("sp", "tp"),
            P("sp", "tp"),
        ),
        out_specs=P(("sp", "tp"), None),
        check_vma=False,
    )
```

profile of v0, /device:TPU:0, one launch (start us, length us, event | category | flops | bytes accessed | tf_op | source)
XLA Modules:
  0.0 639.9 jit_solution(16293472215441492424)
XLA Ops:
  14.7 90.1 %all-gather.4.cloned.1.call-done = bf16[16384,320]{1,0:T(8,128)(2,1)} async-done(((bf16[1024,320]{1,0:T(8,128)(2,1)}), bf16[16384,320]{1,0:T(8,128)(2,1)}) %all-gather.4.cloned.1.call-update) | async-done | bytes 10485776 | tf_op jit(solution)/shard_map/all_gather | solution.py:16
  104.9 3.7 slice.39
  108.5 4.8 copy.29
  113.3 7.1 %slice.38 = bf16[16384,256]{1,0:T(8,128)(2,1)} slice(bf16[16384,320]{1,0:T(8,128)(2,1)} %all-gather.4.cloned.1.call-done), slice={[0:16384], [0:256]} | slice | bytes 16777216 | tf_op jit(solution)/shard_map/slice | solution.py:18
  122.7 59.4 %while.15 = (s32[]{:T(128)}, f32[2,1024]{1,0:T(2,128)S(1)}, f32[2,1024]{1,0:T(2,128)}, f32[2,1024,128]{2,1,0:T(8,128)}, s32[8]{0:T(128)}, /*index=5*/s32[]{:T(12...) while((s32[]{:T(128)}, f32[2,1024]{1,0:T(2,128)S(1)}, ...), condition=%wide.region_6.7_spmd.clone, body=%wide.region_1.6_spmd.clone.sunk | while | flops 3266845696 | bytes 178161584 | solution.py:109
  124.6 43.7 %conditional.3 = ((f32[2,1024]{1,0:T(2,128)S(1)}, f32[2,1024]{1,0:T(2,128)}, f32[2,1024,128]{2,1,0:T(8,128)})) conditional(s32[]{:T(128)} %convert_element_type.126, (f32[2,1024]{1,0:T(2,128)S(1)}, f32[2,1024]{1,0:T(2,128)}, f32[2,1024,128]{2,1,0:T(8,128)}) %tuple.44, (s32[]{:T(128)}, s32[]{:T(128)}, bf16[8,2048,256]{2,1,0:T(8,128)(2,1)}, s32[]{:T(128)}, ...), branch_computations={%region_2.2_spmd, %region_3.5_spmd} | conditional | flops 3266845696 | bytes 178157184 | solution.py:107
  124.6 1.8 convolution_convert_fusion.1
  126.4 8.1 %fusion.37 = f32[2,2048,1024]{2,1,0:T(8,128)} fusion(bf16[2048,2,128]{0,2,1:T(8,128)(2,1)S(1)} %bitcast.42, bf16[1024,2,128]{2,0,1:T(8,128)(2,1)S(1)} %get-tuple-element.152), kind=kOutput, calls=%fused_computation.62 | convolution fusion | flops 1073741824 | bytes 18350080 | tf_op jit(solution)/shard_map/while/body/eval_jaxpr/cond/branch_1_fun/qhd,khd->hqk/dot_general | solution.py:66
  134.5 1.3 broadcast_compare_fusion
  135.9 12.3 %fusion.36 = (f32[2,1024]{1,0:T(2,128)S(1)}, f32[2,1024,2048]{1,2,0:T(8,128)}) fusion(bf16[1024,2,64]{0,2,1:T(8,128)(2,1)} %get-tuple-element.154, bf16[8,2048,64]{1,2,0:T(8,128)(2,1)} %get-tuple-element.153, s32[]{:T(128)} %get-tuple-element.150, f32[2,2048,1024]{2,1,0:T(8,128)} %fusion.37, pred[1024,2048]{0,1:T(8,128)(4,1)S(1)} %broadcast_compare_fusion), kind=kOutput, calls=%fused_computation.61 | convolution fusion | flops 553646080 | bytes 36184576 | tf_op jit(solution)/shard_map/while/body/eval_jaxpr/cond/branch_1_fun/qhr,kr->hqk/dot_general | solution.py:67
  148.2 8.6 %fusion.5 = f32[2,1024]{1,0:T(2,128)S(1)} fusion(f32[2,1024,2048]{1,2,0:T(8,128)} %get-tuple-element.256, f32[2,1024]{1,0:T(2,128)S(1)} %max.4, pred[1024,2048]{0,1:T(8,128)(4,1)} %copy-done.2), kind=kLoop, calls=%fused_computation.6 | loop fusion | flops 12580864 | bytes 18890752 | tf_op jit(solution)/shard_map/while/body/eval_jaxpr/cond/branch_1_fun/reduce_sum | solution.py:74
  156.8 2.1 multiply_add_fusion
  158.9 1.8 convolution_convert_fusion
  160.6 7.7 %fusion.9 = f32[2,1024,128]{2,1,0:T(8,128)} fusion(bf16[2048,2,128]{0,2,1:T(8,128)(2,1)S(1)} %bitcast.44, f32[2,1024,2048]{1,2,0:T(8,128)S(1)} %copy-done.1, f32[2,1024]{1,0:T(2,128)S(1)} %max.4, pred[1024,2048]{0,1:T(8,128)(4,1)} %copy-done.2, f32[2,1024,128]{2,1,0:T(8,128)} %get-tuple-element.156, f32[2,1024]{1,0:T(2,128)S(1)} %get-tuple-element.254), kind=kOutput, calls=%fused_computation.12 | convolution fusion | flops 1086849024 | bytes 22036480 | tf_op jit(solution)/shard_map/while/body/eval_jaxpr/cond/branch_1_fun/hqk,khd->hqd/dot_general | solution.py:75
  174.2 1.3 dynamic_slice.38
  176.2 1.3 dynamic_slice.38
  178.1 1.3 dynamic_slice.38
  182.1 2.5 bitcast_convert_fusion
  184.6 53.7 %all_to_all.5 = bf16[8,128,2048]{2,1,0:T(8,128)(2,1)S(1)} all-to-all(bf16[8,128,2048]{2,1,0:T(8,128)(2,1)S(1)} %bitcast.46), channel_id=1, replica_groups=mesh['sp'=16,'tp'=8] {'tp'}, dimensions={0} | all-to-all | bytes 8388608 | tf_op jit(solution)/shard_map/all_to_all | solution.py:31
  240.7 332.6 %all-gather.6.cloned.1.call-done = bf16[1024,2048]{1,0:T(8,128)(2,1)} async-done(((bf16[128,2048]{1,0:T(8,128)(2,1)}), bf16[1024,2048]{1,0:T(8,128)(2,1)}) %all-gather.6.cloned.1.call-update) | async-done | bytes 4194320 | tf_op jit(solution)/shard_map/all_gather | solution.py:187
  573.4 7.9 %fusion.25 = f32[1024,704]{0,1:T(8,128)} fusion(bf16[1024,2048]{1,0:T(8,128)(2,1)} %all-gather.6.cloned.1.call-done, bf16[2048,2112]{0,1:T(8,128)(2,1)} %all-gather.8.cloned.1.call-done), kind=kOutput, calls=%fused_computation.33 | convolution fusion | flops 2952790016 | bytes 9961472 | tf_op jit(solution)/shard_map/dot_general | solution.py:188
  581.3 12.0 %convolution_convert_fusion.2 = bf16[1024,2048]{1,0:T(8,128)(2,1)} fusion(bf16[2048,2112]{0,1:T(8,128)(2,1)} %all-gather.8.cloned.1.call-done, f32[1024,704]{0,1:T(8,128)} %fusion.25, bf16[1024,2048]{1,0:T(8,128)(2,1)} %all-gather.6.cloned.1.call-done), kind=kOutput, calls=%fused_computation.29 | convolution fusion | flops 5912002560 | bytes 17039360 | tf_op jit(solution)/shard_map/dot_general | solution.py:192
  593.3 38.0 %reduce-scatter.2.cloned.1.call-done = bf16[128,2048]{1,0:T(8,128)(2,1)} async-done(((bf16[1024,2048]{1,0:T(8,128)(2,1)}), bf16[128,2048]{1,0:T(8,128)(2,1)}) %reduce-scatter.2.cloned.1.call-update) | async-done | bytes 524304 | tf_op jit(solution)/shard_map/reduce_scatter | solution.py:195
  631.3 2.0 add_convert_fusion
  (79 shorter events, 19.1 us)
Async XLA Ops:
  6.5 175.5 %copy-start = (bf16[256,2048]{1,0:T(8,128)(2,1)S(1)}, bf16[256,2048]{1,0:T(8,128)(2,1)}, u32[]{:S(2)}) copy-start(bf16[256,2048]{1,0:T(8,128)(2,1)} %param.25) | copy-start | bytes 3145732
  6.5 5.8 copy-start.9
  6.5 5.8 copy-start.8
  6.5 5.8 copy-start.7
  6.5 6.7 %copy-start.6 = (bf16[1024,128]{1,0:T(8,128)(2,1)S(1)}, bf16[1024,128]{1,0:T(8,128)(2,1)}, u32[]{:S(2)}) copy-start(bf16[1024,128]{1,0:T(8,128)(2,1)} %param.19) | copy-start | bytes 786436
  6.5 6.9 %copy-start.5 = (bf16[1024,256]{1,0:T(8,128)(2,1)S(1)}, bf16[1024,256]{1,0:T(8,128)(2,1)}, u32[]{:S(2)}) copy-start(bf16[1024,256]{1,0:T(8,128)(2,1)} %param.18) | copy-start | bytes 1572868
  6.6 98.3 %all-gather.4.cloned.1.call-start = ((), (), s32[]{:S(2)}) async-start(), calls=%async_computation.2 | async-start | bytes 13369344 | tf_op jit(solution)/shard_map/all_gather | solution.py:16
  12.3 228.4 %all-gather.8.cloned.1.call-start = ((), (), s32[]{:S(2)}) async-start(), calls=%async_computation.4 | async-start | bytes 9191424 | tf_op jit(solution)/shard_map/all_gather | solution.py:16
  13.2 560.1 %all-gather.6.cloned.1.call-start = ((), (), s32[]{:S(2)}) async-start(), calls=%async_computation.3 | async-start | bytes 4718592 | tf_op jit(solution)/shard_map/all_gather | solution.py:187
  135.9 12.3 %copy-start.2 = (pred[1024,2048]{0,1:T(8,128)(4,1)}, pred[1024,2048]{0,1:T(8,128)(4,1)S(1)}, u32[]{:S(2)}) copy-start(pred[1024,2048]{0,1:T(8,128)(4,1)S(1)} %broadcast_compare_fusion) | copy-start | bytes 6291460 | tf_op jit(solution)/shard_map/while/body/eval_jaxpr/cond
  148.2 10.7 %copy-start.4 = (bf16[256,256]{1,0:T(8,128)(2,1)S(1)}, bf16[256,256]{1,0:T(8,128)(2,1)}, u32[]{:S(2)}) copy-start(bf16[256,256]{1,0:T(8,128)(2,1)} %get-tuple-element.157) | copy-start | bytes 393220 | tf_op jit(solution)/shard_map/while/body/eval_jaxpr/cond
  148.2 12.5 %copy-start.1 = (f32[2,1024,2048]{1,2,0:T(8,128)S(1)}, f32[2,1024,2048]{1,2,0:T(8,128)}, u32[]{:S(2)}) copy-start(f32[2,1024,2048]{1,2,0:T(8,128)} %get-tuple-element.256) | copy-start | bytes 50331652 | tf_op jit(solution)/shard_map/while/body/eval_jaxpr/cond
  238.4 1.0 copy-start.3
  238.4 1.3 copy-start.10
  240.6 390.7 %reduce-scatter.2.cloned.1.call-start = ((), (), s32[]{:S(2)}) async-start(), calls=%async_computation.5 | async-start | bytes 4718592 | tf_op jit(solution)/shard_map/reduce_scatter | solution.py:195
Sparse Core Ops, SparseCore 0:
  12.4 92.3 all-gather.3
  107.0 78.2 all-gather.7
  240.7 332.5 all-gather.5
  593.4 37.8 reduce-scatter.1
where the time goes:
time: 641 us; the launch traced here: 640 us
  waiting for transfers between devices  461 us (72%)
  matrix products  54 us (8%)
  blocking collectives  53.7 us (8%)
  local copies, waits for them, and re-layouts  29.4 us (5%)
  other arithmetic  22.9 us (4%)
  between operations  13.3 us (2%)
    all_gather x1, waiting for transfers between devices, on_device(): row_piece = lax.all_gather(normed, 'tp', axis=0, tiled=True)  333 us
    all_gather x2, waiting for transfers between devices, in_one_piece(): lax.all_gather(both, axis, axis=dim, tiled=True)  90.1 us
    all_to_all x1, blocking collectives, summed_on_arrival(): lax.all_to_all(tiles, axis, split_axis=0, concat_axis=0, tiled=True)  53.7 us
    reduce_scatter x1, waiting for transfers between devices, on_device(): lax.psum_scatter(lax.optimization_barrier(down_term.astype(jnp.bfloat16))...  38 us
  transfers between devices with their start and end apart: 4, of which 3 were waited for; matrix products, arithmetic and copies ran while one was open for 12% of the time, Pallas kernels for 0%

commit v1 on v0

--- a/solution.py
+++ b/solution.py
@@ -184,7 +184,9 @@
     )
     stream = resid.astype(jnp.float32) + attention_proj
     normed = rms_scale(stream, mix_gain).astype(jnp.bfloat16)
-    row_piece = lax.all_gather(normed, "tp", axis=0, tiled=True)
+    row_piece = jnp.concatenate(
+        lax.all_to_all(jnp.stack([normed] * lax.axis_size("tp")), "tp", 0, 0), axis=0
+    )
     gate_value = jnp.dot(row_piece, gate_full, preferred_element_type=jnp.float32)
     upward = jnp.dot(row_piece, up_full, preferred_element_type=jnp.float32)
     hidden = (jax.nn.silu(gate_value) * upward).astype(jnp.bfloat16)

time: 641 us -> 663 us (1.034)
  waiting for transfers between devices: 461 us -> 479 us
    all_gather x1 -> x0, waiting for transfers between devices: 333 us -> none  [on_device(): row_piece = lax.all_gather(normed, 'tp', axis=0, tiled=True)]
    reduce_scatter x1, waiting for transfers between devices: 38 us -> 339 us  [on_device(): lax.psum_scatter(lax.optimization_barrier(down_term.astype(jnp.bfloat16))...]
    all_to_all x0 -> x1, waiting for transfers between devices: none -> 49.6 us  [on_device(): lax.all_to_all(jnp.stack([normed] * lax.axis_size('tp')), 'tp', 0, 0)]
where the time goes in v1:
time: 663 us; the launch traced here: 662 us
  waiting for transfers between devices  479 us (72%)
  matrix products  54.1 us (8%)
  blocking collectives  53.7 us (8%)
  local copies, waits for them, and re-layouts  30.8 us (5%)
  other arithmetic  22 us (3%)
  between operations  13.3 us (2%)
    reduce_scatter x1, waiting for transfers between devices, on_device(): lax.psum_scatter(lax.optimization_barrier(down_term.astype(jnp.bfloat16))...  339 us
    all_gather x2, waiting for transfers between devices, in_one_piece(): lax.all_gather(both, axis, axis=dim, tiled=True)  90.2 us
    all_to_all x1, blocking collectives, summed_on_arrival(): lax.all_to_all(tiles, axis, split_axis=0, concat_axis=0, tiled=True)  53.7 us
    all_to_all x1, waiting for transfers between devices, on_device(): lax.all_to_all(jnp.stack([normed] * lax.axis_size('tp')), 'tp', 0, 0)  49.6 us
  transfers between devices with their start and end apart: 4, of which 3 were waited for; matrix products, arithmetic and copies ran while one was open for 12% of the time, Pallas kernels for 0%

profile of v1, /device:TPU:0, one launch (start us, length us, event | category | flops | bytes accessed | tf_op | source)
XLA Modules:
  0.0 662.1 jit_solution(16060458931885874294)
XLA Ops:
  8.6 1.3 fusion.31
  14.7 90.2 %all-gather.3.cloned.1.call-done = bf16[16384,320]{1,0:T(8,128)(2,1)} async-done(((bf16[1024,320]{1,0:T(8,128)(2,1)}), bf16[16384,320]{1,0:T(8,128)(2,1)}) %all-gather.3.cloned.1.call-update) | async-done | bytes 10485776 | tf_op jit(solution)/shard_map/all_gather | solution.py:16
  104.9 3.7 slice.39
  108.6 4.8 copy.29
  113.4 7.1 %slice.38 = bf16[16384,256]{1,0:T(8,128)(2,1)} slice(bf16[16384,320]{1,0:T(8,128)(2,1)} %all-gather.3.cloned.1.call-done), slice={[0:16384], [0:256]} | slice | bytes 16777216 | tf_op jit(solution)/shard_map/slice | solution.py:18
  122.6 57.8 %while.15 = (s32[]{:T(128)}, f32[2,1024]{1,0:T(2,128)S(1)}, f32[2,1024]{1,0:T(2,128)}, f32[2,1024,128]{2,1,0:T(8,128)}, s32[8]{0:T(128)}, /*index=5*/s32[]{:T(12...) while((s32[]{:T(128)}, f32[2,1024]{1,0:T(2,128)S(1)}, ...), condition=%wide.region_6.7_spmd.clone, body=%wide.region_1.6_spmd.clone.sunk | while | flops 3266845696 | bytes 178161584 | solution.py:109
  124.4 43.7 %conditional.3 = ((f32[2,1024]{1,0:T(2,128)S(1)}, f32[2,1024]{1,0:T(2,128)}, f32[2,1024,128]{2,1,0:T(8,128)})) conditional(s32[]{:T(128)} %convert_element_type.126, (f32[2,1024]{1,0:T(2,128)S(1)}, f32[2,1024]{1,0:T(2,128)}, f32[2,1024,128]{2,1,0:T(8,128)}) %tuple.44, (s32[]{:T(128)}, s32[]{:T(128)}, bf16[8,2048,256]{2,1,0:T(8,128)(2,1)}, s32[]{:T(128)}, ...), branch_computations={%region_2.2_spmd, %region_3.5_spmd} | conditional | flops 3266845696 | bytes 178157184 | solution.py:107
  124.4 1.8 convolution_convert_fusion.1
  126.1 8.1 %fusion.37 = f32[2,2048,1024]{2,1,0:T(8,128)} fusion(bf16[2048,2,128]{0,2,1:T(8,128)(2,1)S(1)} %bitcast.43, bf16[1024,2,128]{2,0,1:T(8,128)(2,1)S(1)} %get-tuple-element.152), kind=kOutput, calls=%fused_computation.62 | convolution fusion | flops 1073741824 | bytes 18350080 | tf_op jit(solution)/shard_map/while/body/eval_jaxpr/cond/branch_1_fun/qhd,khd->hqk/dot_general | solution.py:66
  134.3 1.3 broadcast_compare_fusion
  135.6 12.3 %fusion.36 = (f32[2,1024]{1,0:T(2,128)S(1)}, f32[2,1024,2048]{1,2,0:T(8,128)}) fusion(bf16[1024,2,64]{0,2,1:T(8,128)(2,1)} %get-tuple-element.154, bf16[8,2048,64]{1,2,0:T(8,128)(2,1)} %get-tuple-element.153, s32[]{:T(128)} %get-tuple-element.150, f32[2,2048,1024]{2,1,0:T(8,128)} %fusion.37, pred[1024,2048]{0,1:T(8,128)(4,1)S(1)} %broadcast_compare_fusion), kind=kOutput, calls=%fused_computation.61 | convolution fusion | flops 553646080 | bytes 36184576 | tf_op jit(solution)/shard_map/while/body/eval_jaxpr/cond/branch_1_fun/qhr,kr->hqk/dot_general | solution.py:67
  148.0 8.6 %fusion.5 = f32[2,1024]{1,0:T(2,128)S(1)} fusion(f32[2,1024,2048]{1,2,0:T(8,128)} %get-tuple-element.256, f32[2,1024]{1,0:T(2,128)S(1)} %max.4, pred[1024,2048]{0,1:T(8,128)(4,1)} %copy-done.2), kind=kLoop, calls=%fused_computation.6 | loop fusion | flops 12580864 | bytes 18890752 | tf_op jit(solution)/shard_map/while/body/eval_jaxpr/cond/branch_1_fun/reduce_sum | solution.py:74
  156.6 2.0 multiply_add_fusion
  158.6 1.8 convolution_convert_fusion
  160.4 7.7 %fusion.9 = f32[2,1024,128]{2,1,0:T(8,128)} fusion(bf16[2048,2,128]{0,2,1:T(8,128)(2,1)S(1)} %bitcast.45, f32[2,1024,2048]{1,2,0:T(8,128)S(1)} %copy-done.1, f32[2,1024]{1,0:T(2,128)S(1)} %max.4, pred[1024,2048]{0,1:T(8,128)(4,1)} %copy-done.2, f32[2,1024,128]{2,1,0:T(8,128)} %get-tuple-element.156, f32[2,1024]{1,0:T(2,128)S(1)} %get-tuple-element.254), kind=kOutput, calls=%fused_computation.12 | convolution fusion | flops 1086849024 | bytes 22036480 | tf_op jit(solution)/shard_map/while/body/eval_jaxpr/cond/branch_1_fun/hqk,khd->hqd/dot_general | solution.py:75
  180.4 2.5 bitcast_convert_fusion
  183.0 53.7 %all_to_all.10 = bf16[8,128,2048]{2,1,0:T(8,128)(2,1)S(1)} all-to-all(bf16[8,128,2048]{2,1,0:T(8,128)(2,1)S(1)} %bitcast.47), channel_id=1, replica_groups=mesh['sp'=16,'tp'=8] {'tp'}, dimensions={0} | all-to-all | bytes 8388608 | tf_op jit(solution)/shard_map/all_to_all | solution.py:31
  238.2 2.5 stack.2
  240.7 4.6 all-to-all-start.1
  245.3 49.6 %all-to-all-done.1 = bf16[8,128,2048]{2,1,0:T(8,128)(2,1)} async-done(((bf16[8,128,2048]{2,1,0:T(8,128)(2,1)}), bf16[8,128,2048]{2,1,0:T(8,128)(2,1)}, u32[]{:S(2)}, u32[]{:S(2)}) %all-to-all-start.1) | async-done | bytes 4194336 | tf_op jit(solution)/shard_map/all_to_all | solution.py:188
  294.9 7.9 %fusion.25 = f32[1024,704]{0,1:T(8,128)} fusion(bf16[1024,2048]{1,0:T(8,128)(2,1)} %bitcast.14, bf16[2048,2112]{0,1:T(8,128)(2,1)} %all-gather.5.cloned.1.call-done), kind=kOutput, calls=%fused_computation.33 | convolution fusion | flops 2952790016 | bytes 9961472 | tf_op jit(solution)/shard_map/dot_general | solution.py:190
  302.8 12.0 %convolution_convert_fusion.2 = bf16[1024,2048]{1,0:T(8,128)(2,1)} fusion(bf16[2048,2112]{0,1:T(8,128)(2,1)} %all-gather.5.cloned.1.call-done, f32[1024,704]{0,1:T(8,128)} %fusion.25, bf16[1024,2048]{1,0:T(8,128)(2,1)} %bitcast.14), kind=kOutput, calls=%fused_computation.29 | convolution fusion | flops 5912002560 | bytes 17039360 | tf_op jit(solution)/shard_map/dot_general | solution.py:194
  314.8 338.7 %reduce-scatter.2.cloned.1.call-done = bf16[128,2048]{1,0:T(8,128)(2,1)} async-done(((bf16[1024,2048]{1,0:T(8,128)(2,1)}), bf16[128,2048]{1,0:T(8,128)(2,1)}) %reduce-scatter.2.cloned.1.call-update) | async-done | bytes 524304 | tf_op jit(solution)/shard_map/reduce_scatter | solution.py:197
  653.6 2.0 add_convert_fusion
  (79 shorter events, 19.7 us)
Async XLA Ops:
  6.5 173.9 %copy-start = (bf16[256,2048]{1,0:T(8,128)(2,1)S(1)}, bf16[256,2048]{1,0:T(8,128)(2,1)}, u32[]{:S(2)}) copy-start(bf16[256,2048]{1,0:T(8,128)(2,1)} %param.25) | copy-start | bytes 3145732
  6.5 5.8 copy-start.9
  6.5 5.8 copy-start.8
  6.5 5.8 copy-start.7
  6.5 6.7 %copy-start.6 = (bf16[1024,128]{1,0:T(8,128)(2,1)S(1)}, bf16[1024,128]{1,0:T(8,128)(2,1)}, u32[]{:S(2)}) copy-start(bf16[1024,128]{1,0:T(8,128)(2,1)} %param.19) | copy-start | bytes 786436
  6.5 6.9 %copy-start.5 = (bf16[1024,256]{1,0:T(8,128)(2,1)S(1)}, bf16[1024,256]{1,0:T(8,128)(2,1)}, u32[]{:S(2)}) copy-start(bf16[1024,256]{1,0:T(8,128)(2,1)} %param.18) | copy-start | bytes 1572868
  6.6 98.3 %all-gather.3.cloned.1.call-start = ((), (), s32[]{:S(2)}) async-start(), calls=%async_computation.3 | async-start | bytes 13369344 | tf_op jit(solution)/shard_map/all_gather | solution.py:16
  12.3 233.0 %all-gather.5.cloned.1.call-start = ((), (), s32[]{:S(2)}) async-start(), calls=%async_computation.4 | async-start | bytes 9191424 | tf_op jit(solution)/shard_map/all_gather | solution.py:16
  135.6 12.3 %copy-start.2 = (pred[1024,2048]{0,1:T(8,128)(4,1)}, pred[1024,2048]{0,1:T(8,128)(4,1)S(1)}, u32[]{:S(2)}) copy-start(pred[1024,2048]{0,1:T(8,128)(4,1)S(1)} %broadcast_compare_fusion) | copy-start | bytes 6291460 | tf_op jit(solution)/shard_map/while/body/eval_jaxpr/cond
  147.9 10.7 %copy-start.4 = (bf16[256,256]{1,0:T(8,128)(2,1)S(1)}, bf16[256,256]{1,0:T(8,128)(2,1)}, u32[]{:S(2)}) copy-start(bf16[256,256]{1,0:T(8,128)(2,1)} %get-tuple-element.157) | copy-start | bytes 393220 | tf_op jit(solution)/shard_map/while/body/eval_jaxpr/cond
  147.9 12.4 %copy-start.1 = (f32[2,1024,2048]{1,2,0:T(8,128)S(1)}, f32[2,1024,2048]{1,2,0:T(8,128)}, u32[]{:S(2)}) copy-start(f32[2,1024,2048]{1,2,0:T(8,128)} %get-tuple-element.256) | copy-start | bytes 50331652 | tf_op jit(solution)/shard_map/while/body/eval_jaxpr/cond
  236.7 1.0 copy-start.3
  236.7 1.3 copy-start.10
  240.7 54.2 %all-to-all-start.1 = ((bf16[8,128,2048]{2,1,0:T(8,128)(2,1)}), bf16[8,128,2048]{2,1,0:T(8,128)(2,1)}, u32[]{:S(2)}, u32[]{:S(2)}) async-start(bf16[8,128,2048]{2,1,0:T(8,128)(2,1)} %stack.2), calls=%async_computation.1 | async-start | bytes 8388608 | tf_op jit(solution)/shard_map/all_to_all | solution.py:188
  245.3 408.3 %reduce-scatter.2.cloned.1.call-start = ((), (), s32[]{:S(2)}) async-start(), calls=%async_computation.5 | async-start | bytes 4718592 | tf_op jit(solution)/shard_map/reduce_scatter | solution.py:197
Sparse Core Ops, SparseCore 0:
  12.4 92.3 all-gather.2
  107.0 78.2 all-gather.4
  315.0 338.5 reduce-scatter.1
